TPU v7x, 32 devices: a whole 2x2x4 slice. The times are simulated.
32 devices in a mesh: ep: 8 (over z, y), tp: 4 (over x, core).
Axes of the slice: x: 2, y: 2, z: 4, core: 2. Of those that a mesh axis runs over, the one named last changes fastest.
Arguments:
- queries_a: bfloat16 [1024, 1024], P('ep', 'tp'), may hold values from -128 to 128
- queries_b: bfloat16 [1024, 1024], P('ep', 'tp'), may hold values from -128 to 128
- keys_a: bfloat16 [1024, 512], P('ep', 'tp'), may hold values from -8 to 8
- keys_b: bfloat16 [1024, 512], P('ep', 'tp'), may hold values from -8 to 8
- values: bfloat16 [1024, 1024], P('ep', 'tp'), may hold values from -6 to 6
- lambdas: float32 [16], P('tp'), may hold values from 0.3 to 0.8
- head_gain: float32 [128], replicated, may hold values from 0.1 to 1.9
- w_out: bfloat16 [2048, 2048], P('tp'), may hold values from -0.125 to 0.125
- moe_tokens: bfloat16 [4096, 2048], P(('ep', 'tp')), may hold values from -80 to 80
- moe_gain: float32 [2048], replicated, may hold values from 0.1 to 1.9
- routes: int32 [4096, 2], P(('ep', 'tp')), may hold values from 0 to 7, all different within a row; in each aligned block of 128 rows (0 to 127, 128 to 255, ...) at most 48 rows name the same one
- route_weights: float32 [4096, 2], P(('ep', 'tp')), may hold values from 0.1 to 1
- w_gate: bfloat16 [8, 2048, 2048], P('ep', None, 'tp'), may hold values from -4 to 4
- w_up: bfloat16 [8, 2048, 2048], P('ep', None, 'tp'), may hold values from -4 to 4
- w_down: bfloat16 [8, 2048, 2048], P('ep', 'tp'), may hold values from -0.0625 to 0.0625
Outputs:
- mixer_out: bfloat16 [1024, 2048], P(('ep', 'tp'))
- moe_out: bfloat16 [4096, 2048], P(('ep', 'tp'))
Inputs may be any that keep to these rules, and one draw needn't show every extreme that they name: `routes`: each row names 2 different experts. Within the rows of one device no expert is named by more than 48 rows, a bound that some block reaches of some device.
All inputs are finite; a program needn't handle non-finite values.
Results may differ from a plain program's by a relative error of at most 0.011.
Values may be sent and summed in bfloat16 or wider, within the bound.
A program may use at most 192 MiB of HBM per device.

v0:
```python
import functools

import jax
import jax.numpy as jnp
from jax import lax
from jax.experimental import pallas as pl
from jax.experimental.pallas import tpu as pltpu
from jax.sharding import PartitionSpec as P

HEAD = 64
VDIM = 128
TOP = 2


eps = 1e-05
alpha_act = 1.702
limit_act = 7.0
negative = -1e30


def clamped_unit(gate, up):
    capped = jnp.minimum(gate, limit_act)
    linear = jnp.clip(up, -limit_act, limit_act)
    return capped * jax.nn.sigmoid(alpha_act * capped) * (linear + 1.0)


def hidden_rows(inputs, gate_matrix, up_matrix):
    gate = jnp.dot(inputs, gate_matrix, preferred_element_type=jnp.float32)
    up = jnp.dot(inputs, up_matrix, preferred_element_type=jnp.float32)
    return clamped_unit(gate, up).astype(jnp.bfloat16)


def pick_rows(table, owner):
    valid = owner < table.shape[0]
    chosen = jnp.take(table, jnp.minimum(owner, table.shape[0] - 1), axis=0)
    return jnp.where(valid[:, None], chosen, jnp.zeros_like(chosen))


def mixer(queries_a, queries_b, keys_a, keys_b, values, lambdas, head_gain, w_out):
    tokens = queries_a.shape[0]
    local_heads = lambdas.shape[0]
    kv_local = keys_a.shape[1] // HEAD
    group = local_heads // kv_local
    scale = HEAD ** (-0.5)
    query_pos = lax.axis_index("ep") * tokens + jnp.arange(tokens, dtype=jnp.int32)
    grouped_a = queries_a.reshape(tokens, kv_local, group, HEAD)
    grouped_b = queries_b.reshape(tokens, kv_local, group, HEAD)
    lowest = jnp.full((kv_local, group, tokens), negative, jnp.float32)
    nothing = jnp.zeros((kv_local, group, tokens), jnp.float32)
    blank = jnp.zeros((kv_local, group, tokens, VDIM), jnp.float32)

    def one_map(grouped, keys, value_rows, visible, state):
        peak, total, accum = state
        scores = (
            jnp.einsum("rgjd,ngd->gjrn", grouped, keys, preferred_element_type=jnp.float32) * scale
        )
        scores = jnp.where(visible, scores, negative)
        new_peak = jnp.maximum(peak, jnp.max(scores, axis=-1))
        expo = jnp.where(visible, jnp.exp(scores - new_peak[..., None]), 0.0)
        total = jnp.sum(expo, axis=-1)
        accum = jnp.einsum(
            "gjrn,ngv->gjrv",
            expo.astype(jnp.bfloat16),
            value_rows,
            preferred_element_type=jnp.float32,
        )
        return (new_peak, total, accum)

    initial = (lowest, nothing, blank, lowest, nothing, blank)
    piece_a = lax.all_gather(keys_a, "ep", axis=0, tiled=True)
    piece_b = lax.all_gather(keys_b, "ep", axis=0, tiled=True)
    piece_v = lax.all_gather(values, "ep", axis=0, tiled=True)
    count = piece_a.shape[0]

    def visit(state):
        key_pos = jnp.arange(count, dtype=jnp.int32)
        visible = key_pos[None, :] <= query_pos[:, None]
        value_rows = piece_v.reshape(count, kv_local, VDIM)
        first = one_map(
            grouped_a, piece_a.reshape(count, kv_local, HEAD), value_rows, visible, state[:3]
        )
        second = one_map(
            grouped_b, piece_b.reshape(count, kv_local, HEAD), value_rows, visible, state[3:]
        )
        return first + second

    result = lax.cond(jnp.int32(0) <= query_pos[tokens - 1], visit, lambda state: state, initial)
    mixed_a = result[2] / result[1][..., None]
    mixed_b = result[5] / result[4][..., None]
    diff = mixed_a - lambdas.reshape(kv_local, group, 1, 1) * mixed_b
    heads_out = (
        diff * lax.rsqrt(jnp.mean(diff * diff, axis=-1, keepdims=True) + eps) * head_gain
    ).astype(jnp.bfloat16)
    weights_out = w_out.reshape(kv_local, group, VDIM, w_out.shape[1])
    return lax.psum_scatter(
        jnp.einsum(
            "gjrv,gjvd->rd", heads_out, weights_out, preferred_element_type=jnp.float32
        ).astype(jnp.bfloat16),
        "tp",
        scatter_dimension=0,
        tiled=True,
    )


def experts(moe_tokens, moe_gain, routes, route_weights, w_gate, w_up, w_down):
    tok_rows, width = moe_tokens.shape
    n_experts = lax.axis_size("ep") * w_gate.shape[0]
    capacity = max(2, 3 * tok_rows * TOP // (2 * n_experts))
    inputs = moe_tokens.astype(jnp.float32)
    normed = (
        inputs * lax.rsqrt(jnp.mean(inputs * inputs, axis=-1, keepdims=True) + eps) * moe_gain
    ).astype(jnp.bfloat16)
    chosen = routes.reshape(-1)
    member = (chosen[:, None] == jnp.arange(n_experts, dtype=jnp.int32)[None, :]).astype(jnp.int32)
    order_in = jnp.sum(jnp.cumsum(member, axis=0) * member, axis=1) - 1
    slot_ids = chosen * capacity + order_in
    owner = (
        jnp.full((n_experts * capacity,), tok_rows, jnp.int32)
        .at[slot_ids]
        .set(jnp.arange(tok_rows * TOP, dtype=jnp.int32) // TOP)
    )
    outgoing = pick_rows(normed, owner).reshape(n_experts, capacity, width)
    arrived = lax.all_to_all(outgoing, "ep", split_axis=0, concat_axis=1, tiled=True).reshape(
        -1, width
    )
    hidden = hidden_rows(lax.all_gather(arrived, "tp", axis=0, tiled=True), w_gate[0], w_up[0])
    expert_out = lax.psum_scatter(
        jnp.dot(hidden, w_down[0], preferred_element_type=jnp.float32).astype(jnp.bfloat16),
        "tp",
        scatter_dimension=0,
        tiled=True,
    )
    returned = lax.all_to_all(
        expert_out.reshape(-1, capacity, width), "ep", split_axis=0, concat_axis=0, tiled=True
    )
    picked = jnp.take(returned.reshape(-1, width), slot_ids, axis=0).reshape(tok_rows, TOP, width)
    return jnp.sum(picked.astype(jnp.float32) * route_weights[:, :, None], axis=1).astype(
        jnp.bfloat16
    )


def body(
    queries_a,
    queries_b,
    keys_a,
    keys_b,
    values,
    lambdas,
    head_gain,
    w_out,
    moe_tokens,
    moe_gain,
    routes,
    route_weights,
    w_gate,
    w_up,
    w_down,
):
    mixer_out = mixer(queries_a, queries_b, keys_a, keys_b, values, lambdas, head_gain, w_out)
    moe_out = experts(moe_tokens, moe_gain, routes, route_weights, w_gate, w_up, w_down)
    return (mixer_out, moe_out)


MESH = pl.DeviceIdType.MESH
OUT, CORE, ACROSS, CORE_ACROSS, PART, PAIR, SUMS, BACK, KV_Z, KV_Y, MIX = range(11)


def xor(first, second, limit):
    total, bit = 0, 1
    while bit < limit:
        total = total + (first // bit + second // bit) % 2 * bit
        bit *= 2
    return total


def exchange(
    n, tokens_in, moe_gain, routes, route_weights, kv, queries_a, queries_b, head_gain, lambdas, w_gate, w_up, w_down, w_out,
    moe_out, mixer_out,
    ret, outgoing, chosen, rows, parts, part_in, pair_in, sums_in, sums, final, hidden, gate_v, up_v, down_v, out_v,
    kv_all, heads, shares, landed, send, recv, local,
):
    me = lax.axis_index("ep")
    tp = lax.axis_index("tp")
    core = tp + 1 - 2 * (tp % 2)
    across = tp + 2 - 4 * (tp // 2)
    cap, width = outgoing.shape[1:]
    units = hidden.shape[1]
    flat = 4 * cap

    def mask_of(k):
        return 2 * ((n // 2 - k // 2) % (n // 2)) + k % 2

    def partner(k):
        return xor(me, mask_of(k), n)

    def copy(kind, k, source, target, device):
        return pltpu.make_async_remote_copy(
            src_ref=source,
            dst_ref=target,
            send_sem=send.at[kind, k],
            recv_sem=recv.at[kind, k],
            device_id=device,
            device_id_type=MESH,
        )

    def out_copy(k):
        return copy(OUT, k, outgoing.at[partner(k)], rows.at[k, 0], {"ep": partner(k)})

    def core_copy(k):
        return copy(CORE, k, rows.at[k, 0], rows.at[k, 1], {"tp": core})

    def across_copy(k):
        return copy(ACROSS, k, rows.at[k, 0], rows.at[k, 2], {"tp": across})

    def core_across_copy(k):
        return copy(CORE_ACROSS, k, rows.at[k, 2], rows.at[k, 3], {"tp": core})

    def part_copy(k):
        return copy(PART, k, parts.at[k, 1], part_in.at[k], {"tp": core})

    def pair_copy(k):
        return copy(PAIR, k, parts.at[k, 3], pair_in.at[k], {"tp": core})

    def sums_copy(k):
        return copy(SUMS, k, sums.at[k], sums_in.at[k], {"tp": across})

    def back_copy(k):
        return copy(BACK, k, final.at[k], ret.at[me], {"ep": partner(k)})

    def kv_z_copy(z):
        return copy(KV_Z, z, kv, kv_all.at[me], {"ep": xor(me, 2 * z, n)})

    def kv_y_copy(z):
        source = xor(me, 2 * z, n)
        return copy(KV_Y, z, kv_all.at[source], kv_all.at[source], {"ep": xor(me, 1, n)})

    def mix_copy(shift):
        target = (tp + shift) % 4
        return copy(MIX, shift, shares.at[target], landed.at[shift - 1], {"tp": target})

    tokens = kv.shape[0]
    local_heads = heads.shape[1] // VDIM
    kv_local = kv.shape[1] // (2 * HEAD + VDIM)
    span = kv_local * HEAD

    def one_map(queries, head, offset):
        g = head // (local_heads // kv_local)
        count = n * tokens
        first = offset + g * HEAD
        keys = kv_all[:, :, first : first + HEAD].reshape(count, HEAD)
        first = 2 * span + g * VDIM
        value_rows = kv_all[:, :, first : first + VDIM].reshape(count, VDIM)
        scores = lax.dot_general(
            queries[:, head * HEAD : (head + 1) * HEAD],
            keys,
            (((1,), (1,)), ((), ())),
            preferred_element_type=jnp.float32,
        ) * HEAD ** (-0.5)
        query_pos = me * tokens + lax.broadcasted_iota(jnp.int32, scores.shape, 0)
        key_pos = lax.broadcasted_iota(jnp.int32, scores.shape, 1)
        scores = jnp.where(key_pos <= query_pos, scores, negative)
        expo = jnp.exp(scores - jnp.max(scores, axis=1, keepdims=True))
        total = jnp.sum(expo, axis=1, keepdims=True)
        mixed = jnp.dot(
            expo.astype(jnp.bfloat16), value_rows, preferred_element_type=jnp.float32
        )
        return mixed / total

    def attend(head):
        diff = one_map(queries_a, head, 0) - lambdas[head] * one_map(queries_b, head, span)
        norm = lax.rsqrt(jnp.mean(diff * diff, axis=1, keepdims=True) + eps)
        heads[:, head * VDIM : (head + 1) * VDIM] = (diff * norm * head_gain[...]).astype(
            jnp.bfloat16
        )

    own_kv = pltpu.make_async_copy(kv, kv_all.at[me], local.at[1])
    own_kv.start()
    loads = [
        pltpu.make_async_copy(w_gate, gate_v, local.at[2]),
        pltpu.make_async_copy(w_up, up_v, local.at[3]),
        pltpu.make_async_copy(w_down, down_v, local.at[4]),
        pltpu.make_async_copy(w_out, out_v, local.at[5]),
    ]
    for load in loads:
        load.start()

    barrier = pltpu.get_barrier_semaphore()
    for shift in range(1, n):
        pl.semaphore_signal(
            barrier, inc=1, device_id={"ep": (me + shift) % n}, device_id_type=MESH
        )
    for shift in range(1, 4):
        pl.semaphore_signal(
            barrier, inc=1, device_id={"tp": (tp + shift) % 4}, device_id_type=MESH
        )

    inputs = tokens_in[...].astype(jnp.float32)
    normed = (
        inputs
        * lax.rsqrt(jnp.mean(inputs * inputs, axis=1, keepdims=True) + eps)
        * moe_gain[...]
    ).astype(jnp.bfloat16)
    count = tokens_in.shape[0]
    expert = lax.broadcasted_iota(jnp.int32, (n, count), 0)
    named = [routes[k : k + 1, :] == expert for k in range(TOP)]
    member = named[0]
    for k in range(1, TOP):
        member = member | named[k]
    earlier = lax.broadcasted_iota(jnp.int32, (count, count), 0) < lax.broadcasted_iota(
        jnp.int32, (count, count), 1
    )
    place = jnp.dot(
        jnp.where(member, 1.0, 0.0).astype(jnp.bfloat16),
        jnp.where(earlier, 1.0, 0.0).astype(jnp.bfloat16),
        preferred_element_type=jnp.float32,
    )
    position = lax.broadcasted_iota(jnp.int32, (cap, count), 0).astype(jnp.float32)
    slots = [jnp.where(named[k], place, -1.0) for k in range(TOP)]
    slot = jnp.where(member, place, -1.0)
    for e in range(n):
        for k in range(TOP):
            chosen[k, e] = jnp.where(slots[k][e : e + 1, :] == position, 1.0, 0.0).astype(
                jnp.bfloat16
            )
        pick = jnp.where(slot[e : e + 1, :] == position, 1.0, 0.0).astype(jnp.bfloat16)
        outgoing[e] = jnp.dot(pick, normed, preferred_element_type=jnp.float32).astype(
            jnp.bfloat16
        )
    rows[0, 0] = outgoing[me]
    pl.semaphore_wait(barrier, n + 2)

    core_copy(0).start()
    across_copy(0).start()

    for k in range(1, 4):
        out_copy(k).start()
    for z in range(1, n // 2):
        kv_z_copy(z).start()

    @pl.loop(4, n)
    def _(k):
        out_copy(k).start()

    own_kv.wait()
    for load in loads:
        load.wait()

    @pl.loop(0, n + 2)
    def _(k):
        @pl.when(k + 1 < n)
        def _():
            out_copy(k + 1).wait_recv()
            core_copy(k + 1).start()
            across_copy(k + 1).start()

        @pl.when(k < n)
        def _():
            across_copy(k).wait_recv()
            core_across_copy(k).start()

        @pl.when((k >= 1) & (k <= n))
        def _():
            j = k - 1
            pair_copy(j).wait_recv()
            sums[j] = (
                parts[j, 2].astype(jnp.float32) + pair_in[j].astype(jnp.float32)
            ).astype(jnp.bfloat16)
            sums_copy(j).start()

        @pl.when(k >= 2)
        def _():
            j = k - 2
            part_copy(j).wait_recv()
            sums_copy(j).wait_recv()
            final[j] = (
                parts[j, 0].astype(jnp.float32)
                + part_in[j].astype(jnp.float32)
                + sums_in[j].astype(jnp.float32)
            ).astype(jnp.bfloat16)

            @pl.when(j >= 1)
            def _():
                back_copy(j).start()

        @pl.when(k < n)
        def _():
            core_copy(k).wait_recv()
            core_across_copy(k).wait_recv()
            inputs = rows[k].reshape(flat, width)
            step = min(256, units)
            for first in range(0, units, step):
                gate = jnp.dot(
                    inputs, gate_v[:, first : first + step], preferred_element_type=jnp.float32
                )
                up = jnp.dot(
                    inputs, up_v[:, first : first + step], preferred_element_type=jnp.float32
                )
                hidden[:, first : first + step] = clamped_unit(gate, up).astype(jnp.bfloat16)
            for first in range(0, width, 256):
                piece = jnp.dot(
                    hidden[...], down_v[:, first : first + 256], preferred_element_type=jnp.float32
                )
                parts[k, :, :, first : first + 256] = piece.astype(jnp.bfloat16).reshape(
                    4, cap, 256
                )
            pair_copy(k).start()
            part_copy(k).start()

        @pl.when(k == n // 4)
        def _():
            for z in range(n // 2):
                if z:
                    kv_z_copy(z).wait_recv()
                kv_y_copy(z).start()

        @pl.when(k == n // 4 + 1)
        def _():
            for z in range(n // 2):
                kv_y_copy(z).wait_recv()

        for turn in range(4):

            @pl.when(k == n // 4 + 1 + turn)
            def _():
                for head in range(turn, local_heads, 4):
                    attend(head)

        @pl.when(k == n // 4 + 5)
        def _():
            for first in range(0, width, 256):
                piece = jnp.dot(
                    heads[...], out_v[:, first : first + 256], preferred_element_type=jnp.float32
                )
                shares[:, :, first : first + 256] = piece.astype(jnp.bfloat16).reshape(
                    4, tokens // 4, 256
                )
            for shift in range(1, 4):
                mix_copy(shift).start()

    ret[me] = final[0]
    total = shares[tp].astype(jnp.float32)
    for shift in range(1, 4):
        mix_copy(shift).wait_recv()
        total = total + landed[shift - 1].astype(jnp.float32)
    mixer_out[...] = total.astype(jnp.bfloat16)
    for shift in range(1, 4):
        mix_copy(shift).wait_send()
    for z in range(n // 2):
        if z:
            kv_z_copy(z).wait_send()
        kv_y_copy(z).wait_send()

    @pl.loop(0, n)
    def _(k):
        for made in (core_copy, across_copy, core_across_copy, part_copy, pair_copy, sums_copy):
            made(k).wait_send()

        @pl.when(k >= 1)
        def _():
            out_copy(k).wait_send()
            back_copy(k).wait_send()
            back_copy(k).wait_recv()

    picks = [chosen[k].reshape(n * cap, count) for k in range(TOP)]
    for first in range(0, width, 256):
        table = ret[:, :, first : first + 256].reshape(n * cap, 256)
        total = 0.0
        for k in range(TOP):
            picked = lax.dot_general(
                picks[k], table, (((0,), (0,)), ((), ())), preferred_element_type=jnp.float32
            )
            total = total + route_weights[:, k : k + 1] * picked
        moe_out[:, first : first + 256] = total.astype(jnp.bfloat16)


def run_exchange(
    n, cap, tokens_in, moe_gain, routes, route_weights, kv, queries_a, queries_b, head_gain,
    lambdas, w_gate, w_up, w_down, w_out,
):
    count, width = tokens_in.shape
    units = w_gate.shape[1]
    block = (n, cap, width)
    vmem = pl.BlockSpec(memory_space=pltpu.VMEM)
    hbm = pl.BlockSpec(memory_space=pl.ANY)
    return pl.pallas_call(
        functools.partial(exchange, n),
        out_shape=(
            jax.ShapeDtypeStruct((count, width), jnp.bfloat16),
            jax.ShapeDtypeStruct((kv.shape[0] // 4, width), jnp.bfloat16),
        ),
        in_specs=[vmem] * 8 + [pl.BlockSpec(memory_space=pltpu.SMEM)] + [hbm] * 4,
        out_specs=(vmem, vmem),
        scratch_shapes=[
            pltpu.VMEM(block, jnp.bfloat16),
            pltpu.VMEM(block, jnp.bfloat16),
            pltpu.VMEM((TOP, n, cap, count), jnp.bfloat16),
            pltpu.VMEM((n, 4, cap, width), jnp.bfloat16),
            pltpu.VMEM((n, 4, cap, width), jnp.bfloat16),
            pltpu.VMEM(block, jnp.bfloat16),
            pltpu.VMEM(block, jnp.bfloat16),
            pltpu.VMEM(block, jnp.bfloat16),
            pltpu.VMEM(block, jnp.bfloat16),
            pltpu.VMEM(block, jnp.bfloat16),
            pltpu.VMEM((4 * cap, units), jnp.bfloat16),
            pltpu.VMEM(w_gate.shape, jnp.bfloat16),
            pltpu.VMEM(w_up.shape, jnp.bfloat16),
            pltpu.VMEM(w_down.shape, jnp.bfloat16),
            pltpu.VMEM(w_out.shape, jnp.bfloat16),
            pltpu.VMEM((n,) + kv.shape, jnp.bfloat16),
            pltpu.VMEM((kv.shape[0], w_out.shape[0]), jnp.bfloat16),
            pltpu.VMEM((4, kv.shape[0] // 4, width), jnp.bfloat16),
            pltpu.VMEM((3, kv.shape[0] // 4, width), jnp.bfloat16),
            pltpu.SemaphoreType.DMA((11, n)),
            pltpu.SemaphoreType.DMA((11, n)),
            pltpu.SemaphoreType.DMA((6,)),
        ],
        compiler_params=pltpu.CompilerParams(
            collective_id=0, has_side_effects=True, vmem_limit_bytes=60 * 2**20
        ),
        name="exchange",
    )(
        tokens_in, moe_gain.reshape(1, -1), routes.T, route_weights,
        kv, queries_a, queries_b, head_gain.reshape(1, -1), lambdas,
        w_gate, w_up, w_down, w_out,
    )


def fast_body(
    queries_a, queries_b, keys_a, keys_b, values, lambdas, head_gain, w_out,
    moe_tokens, moe_gain, routes, route_weights, w_gate, w_up, w_down,
):
    n = lax.axis_size("ep")
    cap = 3 * moe_tokens.shape[0] * TOP // (2 * n)
    kv = jnp.concatenate([keys_a, keys_b, values], axis=1)
    moe_out, mixer_out = run_exchange(
        n, cap, moe_tokens, moe_gain, routes, route_weights, kv, queries_a, queries_b,
        head_gain, lambdas, w_gate[0], w_up[0], w_down[0], w_out,
    )
    return (mixer_out, moe_out)


def whole_body(*args):
    n, n_tp = lax.axis_size("ep"), lax.axis_size("tp")
    tok_rows, w_gate = args[8].shape[0], args[12]
    cap = 3 * tok_rows * TOP // (2 * n)
    if w_gate.shape[0] == 1 and n_tp == 4 and n & (n - 1) == 0 and n >= 8 and cap % 16 == 0:
        return fast_body(*args)
    return body(*args)


def solution(mesh):
    return jax.shard_map(
        whole_body,
        mesh=mesh,
        in_specs=(
            P("ep", "tp"),
            P("ep", "tp"),
            P("ep", "tp"),
            P("ep", "tp"),
            P("ep", "tp"),
            P("tp"),
            P(),
            P("tp", None),
            P(("ep", "tp"), None),
            P(),
            P(("ep", "tp"), None),
            P(("ep", "tp"), None),
            P("ep", None, "tp"),
            P("ep", None, "tp"),
            P("ep", "tp", None),
        ),
        out_specs=(P(("ep", "tp"), None), P(("ep", "tp"), None)),
        check_vma=False,
    )
```

profile of v0, /device:TPU:0, one launch (start us, length us, event | category | flops | bytes accessed | tf_op | source)
XLA Modules:
  0.0 114.6 jit_solution(4233817100735317488)
XLA Ops:
  0.6 1.4 %copy.17.route_weights = f32[128,2]{1,0:T(8,128)} copy(f32[128,2]{0,1:T(2,128)} %param.26) | data formatting | bytes 2048 | tf_op args[11]
  2.0 1.5 %pad_maximum_fusion.kv = bf16[128,512]{1,0:T(8,128)(2,1)} fusion(bf16[128,256]{1,0:T(8,128)(2,1)} %param.19, bf16[128,128]{1,0:T(8,128)(2,1)} %param.18, bf16[128,128]{1,0:T(8,128)(2,1)} %param.17), kind=kLoop, calls=%fused_computation | loop fusion | flops 393216 | bytes 262144 | tf_op jit(solution)/shard_map/concatenate | solution.py:534
  3.6 107.6 %exchange.1 = (bf16[128,2048]{1,0:T(8,128)(2,1)}, bf16[32,2048]{1,0:T(8,128)(2,1)}) custom-call(bf16[128,2048]{1,0:T(8,128)(2,1)} %tokens_in.1, f32[1,2048]{1,0:T(1,128)} %bitcast.9, s32[2,128]{1,0:T(2,128)} %bitcast.10, f32[128,2]{1,0:T(8,128)} %copy.17.route_weights, bf16[128,512]{1,0:T(8,128)(2,1)} %pad_maximum_fusion.kv, bf16[128,256]{1,0:T(8,128)(2,1)} %queries_a.1, ...), custom_call_target="tpu_custom_call" | custom-call | tf_op jit(solution)/shard_map/exchange/pallas_call | solution.py:485
  111.2 1.6 %copy.20 = bf16[32,2048]{1,0:T(8,128)(2,1)} copy(bf16[32,2048]{1,0:T(8,128)(2,1)} %get-tuple-element.8) | data formatting | bytes 262144
  112.7 1.9 %copy.21 = bf16[128,2048]{1,0:T(8,128)(2,1)} copy(bf16[128,2048]{1,0:T(8,128)(2,1)} %get-tuple-element.9) | data formatting | bytes 1048576
where the time goes:
time: 116 us; the launch traced here: 115 us
  Pallas kernels  108 us (93%)
  local copies, waits for them, and re-layouts  4.86 us (4%)
  other arithmetic  1.53 us (1%)
    pallas_call x1, Pallas kernels, run_exchange(): pl.pallas_call(functools.partial(exchange, n), out_shape=(jax.ShapeDtypeS...  108 us
    unnamed x3, local copies, waits for them, and re-layouts  4.86 us

commit v1 on v0

--- a/solution.py
+++ b/solution.py
@@ -174,18 +174,23 @@
 
 
 def exchange(
-    n, tokens_in, moe_gain, routes, route_weights, kv, queries_a, queries_b, head_gain, lambdas, w_gate, w_up, w_down, w_out,
+    n, tokens_in, moe_gain, routes, route_weights, queries_a, queries_b, head_gain, lambdas,
+    keys_a, keys_b, values, w_gate, w_up, w_down, w_out,
     moe_out, mixer_out,
-    ret, outgoing, chosen, rows, parts, part_in, pair_in, sums_in, sums, final, hidden, gate_v, up_v, down_v, out_v,
-    kv_all, heads, shares, landed, send, recv, local,
+    ret, outgoing, weigh, rows, parts, part_in, pair_in, sums_in, sums, final, hidden, gate_v, up_v, down_v, out_v,
+    kv_all, heads, shares, mix_part, mix_pair, mix_in, mix_sum, send, recv, local,
 ):
     me = lax.axis_index("ep")
     tp = lax.axis_index("tp")
     core = tp + 1 - 2 * (tp % 2)
     across = tp + 2 - 4 * (tp // 2)
+    diagonal = core + 2 - 4 * (core // 2)
+    floor, lane = me // 2, me % 2
+    floors = n // 2
     cap, width = outgoing.shape[1:]
     units = hidden.shape[1]
     flat = 4 * cap
+    tokens = kv_all.shape[1]
 
     def mask_of(k):
         return 2 * ((n // 2 - k // 2) % (n // 2)) + k % 2
@@ -227,20 +232,20 @@
     def back_copy(k):
         return copy(BACK, k, final.at[k], ret.at[me], {"ep": partner(k)})
 
-    def kv_z_copy(z):
-        return copy(KV_Z, z, kv, kv_all.at[me], {"ep": xor(me, 2 * z, n)})
-
-    def kv_y_copy(z):
-        source = xor(me, 2 * z, n)
-        return copy(KV_Y, z, kv_all.at[source], kv_all.at[source], {"ep": xor(me, 1, n)})
-
-    def mix_copy(shift):
-        target = (tp + shift) % 4
-        return copy(MIX, shift, shares.at[target], landed.at[shift - 1], {"tp": target})
-
-    tokens = kv.shape[0]
+    def kv_z_copy(stage):
+        block = kv_all.at[2 * (floor - stage + 1) + lane]
+        return copy(KV_Z, stage, block, block, {"ep": me + 2})
+
+    def kv_y_copy(stage):
+        block = kv_all.at[2 * (floor - stage) + lane]
+        return copy(KV_Y, stage, block, block, {"ep": me + 1 - 2 * lane})
+
+    mix_part_copy = copy(MIX, 0, shares.at[core], mix_part, {"tp": core})
+    mix_pair_copy = copy(MIX, 1, shares.at[diagonal], mix_pair, {"tp": core})
+    mix_sum_copy = copy(MIX, 2, mix_sum, mix_in, {"tp": across})
+
     local_heads = heads.shape[1] // VDIM
-    kv_local = kv.shape[1] // (2 * HEAD + VDIM)
+    kv_local = kv_all.shape[2] // (2 * HEAD + VDIM)
     span = kv_local * HEAD
 
     def one_map(queries, head, offset):
@@ -273,16 +278,56 @@
             jnp.bfloat16
         )
 
-    own_kv = pltpu.make_async_copy(kv, kv_all.at[me], local.at[1])
-    own_kv.start()
-    loads = [
-        pltpu.make_async_copy(w_gate, gate_v, local.at[2]),
-        pltpu.make_async_copy(w_up, up_v, local.at[3]),
-        pltpu.make_async_copy(w_down, down_v, local.at[4]),
-        pltpu.make_async_copy(w_out, out_v, local.at[5]),
-    ]
-    for load in loads:
-        load.start()
+    def forward(k):
+        core_copy(k).start()
+        across_copy(k).start()
+
+    def relay(k):
+        across_copy(k).wait_recv()
+        core_across_copy(k).start()
+
+    def send_sums(k):
+        pair_copy(k).wait_recv()
+        sums[k] = (
+            parts[k, 2].astype(jnp.float32) + pair_in[k].astype(jnp.float32)
+        ).astype(jnp.bfloat16)
+        sums_copy(k).start()
+
+    def finish(k):
+        part_copy(k).wait_recv()
+        sums_copy(k).wait_recv()
+        return (
+            parts[k, 0].astype(jnp.float32)
+            + part_in[k].astype(jnp.float32)
+            + sums_in[k].astype(jnp.float32)
+        ).astype(jnp.bfloat16)
+
+    def send_back(k):
+        final[k] = finish(k)
+        back_copy(k).start()
+
+    def feed(k):
+        core_copy(k).wait_recv()
+        core_across_copy(k).wait_recv()
+        inputs = rows[k].reshape(flat, width)
+        step = min(256, units)
+        for first in range(0, units, step):
+            gate = jnp.dot(
+                inputs, gate_v[:, first : first + step], preferred_element_type=jnp.float32
+            )
+            up = jnp.dot(
+                inputs, up_v[:, first : first + step], preferred_element_type=jnp.float32
+            )
+            hidden[:, first : first + step] = clamped_unit(gate, up).astype(jnp.bfloat16)
+        for first in range(0, width, 256):
+            piece = jnp.dot(
+                hidden[...], down_v[:, first : first + 256], preferred_element_type=jnp.float32
+            )
+            parts[k, :, :, first : first + 256] = piece.astype(jnp.bfloat16).reshape(
+                4, cap, 256
+            )
+        pair_copy(k).start()
+        part_copy(k).start()
 
     barrier = pltpu.get_barrier_semaphore()
     for shift in range(1, n):
@@ -293,6 +338,18 @@
         pl.semaphore_signal(
             barrier, inc=1, device_id={"tp": (tp + shift) % 4}, device_id_type=MESH
         )
+
+    loads = [
+        pltpu.make_async_copy(keys_a, kv_all.at[me, :, 0:span], local.at[0]),
+        pltpu.make_async_copy(keys_b, kv_all.at[me, :, span : 2 * span], local.at[1]),
+        pltpu.make_async_copy(values, kv_all.at[me, :, 2 * span :], local.at[2]),
+        pltpu.make_async_copy(w_gate, gate_v, local.at[3]),
+        pltpu.make_async_copy(w_up, up_v, local.at[4]),
+        pltpu.make_async_copy(w_down, down_v, local.at[5]),
+        pltpu.make_async_copy(w_out, out_v, local.at[6]),
+    ]
+    for load in loads:
+        load.start()
 
     inputs = tokens_in[...].astype(jnp.float32)
     normed = (
@@ -315,13 +372,8 @@
         preferred_element_type=jnp.float32,
     )
     position = lax.broadcasted_iota(jnp.int32, (cap, count), 0).astype(jnp.float32)
-    slots = [jnp.where(named[k], place, -1.0) for k in range(TOP)]
     slot = jnp.where(member, place, -1.0)
     for e in range(n):
-        for k in range(TOP):
-            chosen[k, e] = jnp.where(slots[k][e : e + 1, :] == position, 1.0, 0.0).astype(
-                jnp.bfloat16
-            )
         pick = jnp.where(slot[e : e + 1, :] == position, 1.0, 0.0).astype(jnp.bfloat16)
         outgoing[e] = jnp.dot(pick, normed, preferred_element_type=jnp.float32).astype(
             jnp.bfloat16
@@ -329,126 +381,140 @@
     rows[0, 0] = outgoing[me]
     pl.semaphore_wait(barrier, n + 2)
 
-    core_copy(0).start()
-    across_copy(0).start()
-
-    for k in range(1, 4):
-        out_copy(k).start()
-    for z in range(1, n // 2):
-        kv_z_copy(z).start()
-
-    @pl.loop(4, n)
+    forward(0)
+
+    @pl.loop(1, n - 2)
     def _(k):
         out_copy(k).start()
 
-    own_kv.wait()
-    for load in loads:
+    for load in loads[:3]:
         load.wait()
 
-    @pl.loop(0, n + 2)
+    @pl.when(floor < floors - 1)
+    def _():
+        kv_z_copy(1).start()
+
+    for k in range(n - 2, n):
+        out_copy(k).start()
+    kv_y_copy(0).start()
+
+    for other in range(1, floors):
+
+        @pl.when(floor < other)
+        def _():
+            for side in range(2):
+                kv_all[2 * other + side] = jnp.zeros(kv_all.shape[1:], jnp.bfloat16)
+
+    share = route_weights[...]
+    scale = jnp.where(named[0], share[0:1, :], 0.0)
+    for k in range(1, TOP):
+        scale = scale + jnp.where(named[k], share[k : k + 1, :], 0.0)
+    for e in range(n):
+        weight = jnp.where(slot[e : e + 1, :] == position, scale[e : e + 1, :], 0.0)
+        high = weight.astype(jnp.bfloat16)
+        weigh[0, e] = high
+        weigh[1, e] = (weight - high.astype(jnp.float32)).astype(jnp.bfloat16)
+    for load in loads[3:]:
+        load.wait()
+
+    def kv_next(stage):
+        @pl.when(floor >= stage)
+        def _():
+            kv_z_copy(stage).wait_recv()
+            kv_y_copy(stage).start()
+            if stage < floors - 1:
+
+                @pl.when(floor < floors - 1)
+                def _():
+                    kv_z_copy(stage + 1).start()
+
+    @pl.loop(0, n)
     def _(k):
+        @pl.when(k >= 2)
+        def _():
+            send_sums(k - 1)
+
+        @pl.when(k >= 3)
+        def _():
+            send_back(k - 2)
+
         @pl.when(k + 1 < n)
         def _():
             out_copy(k + 1).wait_recv()
-            core_copy(k + 1).start()
-            across_copy(k + 1).start()
-
-        @pl.when(k < n)
-        def _():
-            across_copy(k).wait_recv()
-            core_across_copy(k).start()
-
-        @pl.when((k >= 1) & (k <= n))
-        def _():
-            j = k - 1
-            pair_copy(j).wait_recv()
-            sums[j] = (
-                parts[j, 2].astype(jnp.float32) + pair_in[j].astype(jnp.float32)
-            ).astype(jnp.bfloat16)
-            sums_copy(j).start()
-
-        @pl.when(k >= 2)
-        def _():
-            j = k - 2
-            part_copy(j).wait_recv()
-            sums_copy(j).wait_recv()
-            final[j] = (
-                parts[j, 0].astype(jnp.float32)
-                + part_in[j].astype(jnp.float32)
-                + sums_in[j].astype(jnp.float32)
-            ).astype(jnp.bfloat16)
-
-            @pl.when(j >= 1)
+            forward(k + 1)
+
+        relay(k)
+        feed(k)
+
+        for stage in range(1, floors):
+
+            @pl.when(k == n - floors + stage)
             def _():
-                back_copy(j).start()
-
-        @pl.when(k < n)
-        def _():
-            core_copy(k).wait_recv()
-            core_across_copy(k).wait_recv()
-            inputs = rows[k].reshape(flat, width)
-            step = min(256, units)
-            for first in range(0, units, step):
-                gate = jnp.dot(
-                    inputs, gate_v[:, first : first + step], preferred_element_type=jnp.float32
-                )
-                up = jnp.dot(
-                    inputs, up_v[:, first : first + step], preferred_element_type=jnp.float32
-                )
-                hidden[:, first : first + step] = clamped_unit(gate, up).astype(jnp.bfloat16)
-            for first in range(0, width, 256):
-                piece = jnp.dot(
-                    hidden[...], down_v[:, first : first + 256], preferred_element_type=jnp.float32
-                )
-                parts[k, :, :, first : first + 256] = piece.astype(jnp.bfloat16).reshape(
-                    4, cap, 256
-                )
-            pair_copy(k).start()
-            part_copy(k).start()
-
-        @pl.when(k == n // 4)
-        def _():
-            for z in range(n // 2):
-                if z:
-                    kv_z_copy(z).wait_recv()
-                kv_y_copy(z).start()
-
-        @pl.when(k == n // 4 + 1)
-        def _():
-            for z in range(n // 2):
-                kv_y_copy(z).wait_recv()
-
-        for turn in range(4):
-
-            @pl.when(k == n // 4 + 1 + turn)
-            def _():
-                for head in range(turn, local_heads, 4):
-                    attend(head)
-
-        @pl.when(k == n // 4 + 5)
-        def _():
-            for first in range(0, width, 256):
-                piece = jnp.dot(
-                    heads[...], out_v[:, first : first + 256], preferred_element_type=jnp.float32
-                )
-                shares[:, :, first : first + 256] = piece.astype(jnp.bfloat16).reshape(
-                    4, tokens // 4, 256
-                )
-            for shift in range(1, 4):
-                mix_copy(shift).start()
-
-    ret[me] = final[0]
-    total = shares[tp].astype(jnp.float32)
-    for shift in range(1, 4):
-        mix_copy(shift).wait_recv()
-        total = total + landed[shift - 1].astype(jnp.float32)
-    mixer_out[...] = total.astype(jnp.bfloat16)
-    for shift in range(1, 4):
-        mix_copy(shift).wait_send()
-    for z in range(n // 2):
-        if z:
-            kv_z_copy(z).wait_send()
-        kv_y_copy(z).wait_send()
+                kv_next(stage)
+
+    send_sums(n - 1)
+    send_sums(0)
+    send_back(n - 2)
+    for stage in range(floors):
+
+        @pl.when(floor >= stage)
+        def _():
+            kv_y_copy(stage).wait_recv()
+
+    for head in range(local_heads):
+        attend(head)
+    send_back(n - 1)
+    for first in range(0, width, 256):
+        piece = jnp.dot(
+            heads[...], out_v[:, first : first + 256], preferred_element_type=jnp.float32
+        )
+        shares[:, :, first : first + 256] = piece.astype(jnp.bfloat16).reshape(
+            4, tokens // 4, 256
+        )
+    mix_pair_copy.start()
+    mix_part_copy.start()
+    mix_pair_copy.wait_recv()
+    mix_sum[...] = (
+        shares[across].astype(jnp.float32) + mix_pair[...].astype(jnp.float32)
+    ).astype(jnp.bfloat16)
+    mix_sum_copy.start()
+    ret[me] = finish(0)
+
+    @pl.loop(1, n)
+    def _(k):
+        back_copy(k).wait_recv()
+
+    picks = [weigh[k].reshape(n * cap, count) for k in range(2)]
+    for first in range(0, width, 256):
+        table = ret[:, :, first : first + 256].reshape(n * cap, 256)
+        total = 0.0
+        for k in range(2):
+            total = total + lax.dot_general(
+                picks[k], table, (((0,), (0,)), ((), ())), preferred_element_type=jnp.float32
+            )
+        moe_out[:, first : first + 256] = total.astype(jnp.bfloat16)
+
+    mix_part_copy.wait_recv()
+    mix_sum_copy.wait_recv()
+    mixer_out[...] = (
+        shares[tp].astype(jnp.float32)
+        + mix_part[...].astype(jnp.float32)
+        + mix_in[...].astype(jnp.float32)
+    ).astype(jnp.bfloat16)
+
+    for made in (mix_part_copy, mix_pair_copy, mix_sum_copy):
+        made.wait_send()
+    for stage in range(1, floors):
+
+        @pl.when((floor >= stage - 1) & (floor < floors - 1))
+        def _():
+            kv_z_copy(stage).wait_send()
+
+    for stage in range(floors):
+
+        @pl.when(floor >= stage)
+        def _():
+            kv_y_copy(stage).wait_send()
 
     @pl.loop(0, n)
     def _(k):
@@ -459,41 +525,32 @@
         def _():
             out_copy(k).wait_send()
             back_copy(k).wait_send()
-            back_copy(k).wait_recv()
-
-    picks = [chosen[k].reshape(n * cap, count) for k in range(TOP)]
-    for first in range(0, width, 256):
-        table = ret[:, :, first : first + 256].reshape(n * cap, 256)
-        total = 0.0
-        for k in range(TOP):
-            picked = lax.dot_general(
-                picks[k], table, (((0,), (0,)), ((), ())), preferred_element_type=jnp.float32
-            )
-            total = total + route_weights[:, k : k + 1] * picked
-        moe_out[:, first : first + 256] = total.astype(jnp.bfloat16)
 
 
 def run_exchange(
-    n, cap, tokens_in, moe_gain, routes, route_weights, kv, queries_a, queries_b, head_gain,
-    lambdas, w_gate, w_up, w_down, w_out,
+    n, cap, tokens_in, moe_gain, routes, route_weights, queries_a, queries_b, head_gain,
+    lambdas, keys_a, keys_b, values, w_gate, w_up, w_down, w_out,
 ):
     count, width = tokens_in.shape
     units = w_gate.shape[1]
     block = (n, cap, width)
+    tokens = keys_a.shape[0]
+    kv_width = keys_a.shape[1] + keys_b.shape[1] + values.shape[1]
+    quarter = (tokens // 4, width)
     vmem = pl.BlockSpec(memory_space=pltpu.VMEM)
     hbm = pl.BlockSpec(memory_space=pl.ANY)
     return pl.pallas_call(
         functools.partial(exchange, n),
         out_shape=(
             jax.ShapeDtypeStruct((count, width), jnp.bfloat16),
-            jax.ShapeDtypeStruct((kv.shape[0] // 4, width), jnp.bfloat16),
+            jax.ShapeDtypeStruct(quarter, jnp.bfloat16),
         ),
-        in_specs=[vmem] * 8 + [pl.BlockSpec(memory_space=pltpu.SMEM)] + [hbm] * 4,
+        in_specs=[vmem] * 7 + [pl.BlockSpec(memory_space=pltpu.SMEM)] + [hbm] * 7,
         out_specs=(vmem, vmem),
         scratch_shapes=[
             pltpu.VMEM(block, jnp.bfloat16),
             pltpu.VMEM(block, jnp.bfloat16),
-            pltpu.VMEM((TOP, n, cap, count), jnp.bfloat16),
+            pltpu.VMEM((2, n, cap, count), jnp.bfloat16),
             pltpu.VMEM((n, 4, cap, width), jnp.bfloat16),
             pltpu.VMEM((n, 4, cap, width), jnp.bfloat16),
             pltpu.VMEM(block, jnp.bfloat16),
@@ -506,22 +563,25 @@
             pltpu.VMEM(w_up.shape, jnp.bfloat16),
             pltpu.VMEM(w_down.shape, jnp.bfloat16),
             pltpu.VMEM(w_out.shape, jnp.bfloat16),
-            pltpu.VMEM((n,) + kv.shape, jnp.bfloat16),
-            pltpu.VMEM((kv.shape[0], w_out.shape[0]), jnp.bfloat16),
-            pltpu.VMEM((4, kv.shape[0] // 4, width), jnp.bfloat16),
-            pltpu.VMEM((3, kv.shape[0] // 4, width), jnp.bfloat16),
+            pltpu.VMEM((n, tokens, kv_width), jnp.bfloat16),
+            pltpu.VMEM((tokens, w_out.shape[0]), jnp.bfloat16),
+            pltpu.VMEM((4,) + quarter, jnp.bfloat16),
+            pltpu.VMEM(quarter, jnp.bfloat16),
+            pltpu.VMEM(quarter, jnp.bfloat16),
+            pltpu.VMEM(quarter, jnp.bfloat16),
+            pltpu.VMEM(quarter, jnp.bfloat16),
             pltpu.SemaphoreType.DMA((11, n)),
             pltpu.SemaphoreType.DMA((11, n)),
-            pltpu.SemaphoreType.DMA((6,)),
+            pltpu.SemaphoreType.DMA((7,)),
         ],
         compiler_params=pltpu.CompilerParams(
             collective_id=0, has_side_effects=True, vmem_limit_bytes=60 * 2**20
         ),
         name="exchange",
     )(
-        tokens_in, moe_gain.reshape(1, -1), routes.T, route_weights,
-        kv, queries_a, queries_b, head_gain.reshape(1, -1), lambdas,
-        w_gate, w_up, w_down, w_out,
+        tokens_in, moe_gain.reshape(1, -1), routes.T, route_weights.T,
+        queries_a, queries_b, head_gain.reshape(1, -1), lambdas,
+        keys_a, keys_b, values, w_gate, w_up, w_down, w_out,
     )
 
 
@@ -531,10 +591,9 @@
 ):
     n = lax.axis_size("ep")
     cap = 3 * moe_tokens.shape[0] * TOP // (2 * n)
-    kv = jnp.concatenate([keys_a, keys_b, values], axis=1)
     moe_out, mixer_out = run_exchange(
-        n, cap, moe_tokens, moe_gain, routes, route_weights, kv, queries_a, queries_b,
-        head_gain, lambdas, w_gate[0], w_up[0], w_down[0], w_out,
+        n, cap, moe_tokens, moe_gain, routes, route_weights, queries_a, queries_b,
+        head_gain, lambdas, keys_a, keys_b, values, w_gate[0], w_up[0], w_down[0], w_out,
     )
     return (mixer_out, moe_out)
 

time: 116 us -> 105 us (0.905)
  the two profiles are of different devices: /device:TPU:0 before, /device:TPU:16 now
where the time goes in v1:
time: 105 us
  Pallas kernels  101 us (96%)
  local copies, waits for them, and re-layouts  3.45 us (3%)
    pallas_call x1, Pallas kernels, run_exchange(): pl.pallas_call(functools.partial(exchange, n), out_shape=(jax.ShapeDtypeS...  101 us
    unnamed x2, local copies, waits for them, and re-layouts  3.45 us

profile of v1, /device:TPU:16, one launch (start us, length us, event | category | flops | bytes accessed | tf_op | source)
XLA Modules:
  0.0 105.1 jit_solution(13075203814587397226)
XLA Ops:
  0.6 101.0 %exchange.1 = (bf16[128,2048]{1,0:T(8,128)(2,1)}, bf16[32,2048]{1,0:T(8,128)(2,1)}) custom-call(bf16[128,2048]{1,0:T(8,128)(2,1)} %tokens_in.1, f32[1,2048]{1,0:T(1,128)} %bitcast.10, s32[2,128]{1,0:T(2,128)} %bitcast.11, f32[2,128]{1,0:T(2,128)} %bitcast.12, bf16[128,256]{1,0:T(8,128)(2,1)} %queries_a.1, bf16[128,256]{1,0:T(8,128)(2,1)} %queries_b.1, ...), custom_call_target="tpu_custom_call" | custom-call | tf_op jit(solution)/shard_map/exchange/pallas_call | solution.py:542
  101.6 1.6 %copy.19 = bf16[32,2048]{1,0:T(8,128)(2,1)} copy(bf16[32,2048]{1,0:T(8,128)(2,1)} %get-tuple-element.8) | data formatting | bytes 262144
  103.2 1.9 %copy.20 = bf16[128,2048]{1,0:T(8,128)(2,1)} copy(bf16[128,2048]{1,0:T(8,128)(2,1)} %get-tuple-element.9) | data formatting | bytes 1048576

commit v2 on v1

--- a/solution.py
+++ b/solution.py
@@ -174,9 +174,10 @@
 
 
 def exchange(
-    n, tokens_in, moe_gain, routes, route_weights, queries_a, queries_b, head_gain, lambdas,
+    n, moe_tokens, gain_in, routes_in, weights_in, queries_a_in, queries_b_in, head_gain_in, lambdas_in,
     keys_a, keys_b, values, w_gate, w_up, w_down, w_out,
     moe_out, mixer_out,
+    tokens_in, moe_gain, routes, route_weights, queries_a, queries_b, head_gain, lambdas,
     ret, outgoing, weigh, rows, parts, part_in, pair_in, sums_in, sums, final, hidden, gate_v, up_v, down_v, out_v,
     kv_all, heads, shares, mix_part, mix_pair, mix_in, mix_sum, send, recv, local,
 ):
@@ -193,7 +194,8 @@
     tokens = kv_all.shape[1]
 
     def mask_of(k):
-        return 2 * ((n // 2 - k // 2) % (n // 2)) + k % 2
+        far = k // 2
+        return 2 * ((far + 1) % 3 + 1) * ((far + 3) // 4) + k % 2
 
     def partner(k):
         return xor(me, mask_of(k), n)
@@ -339,17 +341,22 @@
             barrier, inc=1, device_id={"tp": (tp + shift) % 4}, device_id_type=MESH
         )
 
+    pairs = [
+        (moe_tokens, tokens_in), (gain_in, moe_gain), (routes_in, routes),
+        (keys_a, kv_all.at[me, :, 0:span]), (keys_b, kv_all.at[me, :, span : 2 * span]),
+        (values, kv_all.at[me, :, 2 * span :]), (weights_in, route_weights),
+        (w_gate, gate_v), (w_up, up_v), (w_down, down_v), (w_out, out_v),
+        (queries_a_in, queries_a), (queries_b_in, queries_b), (head_gain_in, head_gain),
+        (lambdas_in, lambdas),
+    ]
     loads = [
-        pltpu.make_async_copy(keys_a, kv_all.at[me, :, 0:span], local.at[0]),
-        pltpu.make_async_copy(keys_b, kv_all.at[me, :, span : 2 * span], local.at[1]),
-        pltpu.make_async_copy(values, kv_all.at[me, :, 2 * span :], local.at[2]),
-        pltpu.make_async_copy(w_gate, gate_v, local.at[3]),
-        pltpu.make_async_copy(w_up, up_v, local.at[4]),
-        pltpu.make_async_copy(w_down, down_v, local.at[5]),
-        pltpu.make_async_copy(w_out, out_v, local.at[6]),
+        pltpu.make_async_copy(source, target, local.at[i])
+        for i, (source, target) in enumerate(pairs)
     ]
     for load in loads:
         load.start()
+    for load in loads[:3]:
+        load.wait()
 
     inputs = tokens_in[...].astype(jnp.float32)
     normed = (
@@ -382,19 +389,16 @@
     pl.semaphore_wait(barrier, n + 2)
 
     forward(0)
-
-    @pl.loop(1, n - 2)
-    def _(k):
+    for k in range(1, n // 2):
         out_copy(k).start()
-
-    for load in loads[:3]:
+    for load in loads[3:7]:
         load.wait()
 
     @pl.when(floor < floors - 1)
     def _():
         kv_z_copy(1).start()
 
-    for k in range(n - 2, n):
+    for k in range(n // 2, n):
         out_copy(k).start()
     kv_y_copy(0).start()
 
@@ -409,12 +413,17 @@
     scale = jnp.where(named[0], share[0:1, :], 0.0)
     for k in range(1, TOP):
         scale = scale + jnp.where(named[k], share[k : k + 1, :], 0.0)
-    for e in range(n):
-        weight = jnp.where(slot[e : e + 1, :] == position, scale[e : e + 1, :], 0.0)
-        high = weight.astype(jnp.bfloat16)
-        weigh[0, e] = high
-        weigh[1, e] = (weight - high.astype(jnp.float32)).astype(jnp.bfloat16)
-    for load in loads[3:]:
+    table = jnp.concatenate(
+        [
+            jnp.where(slot[e : e + 1, :] == position, scale[e : e + 1, :], 0.0)
+            for e in range(n)
+        ],
+        axis=0,
+    ).T
+    high = table.astype(jnp.bfloat16)
+    weigh[0] = high
+    weigh[1] = (table - high.astype(jnp.float32)).astype(jnp.bfloat16)
+    for load in loads[7:]:
         load.wait()
 
     def kv_next(stage):
@@ -430,31 +439,42 @@
 
     @pl.loop(0, n)
     def _(k):
-        @pl.when(k >= 2)
+        @pl.when((k >= 2) & (k < 4))
         def _():
             send_sums(k - 1)
-
-        @pl.when(k >= 3)
-        def _():
-            send_back(k - 2)
 
         @pl.when(k + 1 < n)
         def _():
             out_copy(k + 1).wait_recv()
             forward(k + 1)
 
+        @pl.when(k == 4)
+        def _():
+            send_sums(3)
+            send_back(1)
+            kv_next(1)
+
+        @pl.when(k == 5)
+        def _():
+            send_back(2)
+
+        @pl.when(k == 6)
+        def _():
+            send_sums(4)
+            send_back(3)
+            kv_next(2)
+
+        @pl.when(k == 7)
+        def _():
+            send_sums(6)
+            kv_next(3)
+
         relay(k)
         feed(k)
 
-        for stage in range(1, floors):
-
-            @pl.when(k == n - floors + stage)
-            def _():
-                kv_next(stage)
-
-    send_sums(n - 1)
-    send_sums(0)
-    send_back(n - 2)
+    send_sums(7)
+    send_back(4)
+    send_sums(5)
     for stage in range(floors):
 
         @pl.when(floor >= stage)
@@ -463,7 +483,7 @@
 
     for head in range(local_heads):
         attend(head)
-    send_back(n - 1)
+    send_back(6)
     for first in range(0, width, 256):
         piece = jnp.dot(
             heads[...], out_v[:, first : first + 256], preferred_element_type=jnp.float32
@@ -478,20 +498,20 @@
         shares[across].astype(jnp.float32) + mix_pair[...].astype(jnp.float32)
     ).astype(jnp.bfloat16)
     mix_sum_copy.start()
+    send_sums(0)
+    send_back(7)
+    send_back(5)
     ret[me] = finish(0)
 
     @pl.loop(1, n)
     def _(k):
         back_copy(k).wait_recv()
 
-    picks = [weigh[k].reshape(n * cap, count) for k in range(2)]
     for first in range(0, width, 256):
         table = ret[:, :, first : first + 256].reshape(n * cap, 256)
-        total = 0.0
-        for k in range(2):
-            total = total + lax.dot_general(
-                picks[k], table, (((0,), (0,)), ((), ())), preferred_element_type=jnp.float32
-            )
+        total = jnp.dot(weigh[0], table, preferred_element_type=jnp.float32) + jnp.dot(
+            weigh[1], table, preferred_element_type=jnp.float32
+        )
         moe_out[:, first : first + 256] = total.astype(jnp.bfloat16)
 
     mix_part_copy.wait_recv()
@@ -538,19 +558,27 @@
     kv_width = keys_a.shape[1] + keys_b.shape[1] + values.shape[1]
     quarter = (tokens // 4, width)
     vmem = pl.BlockSpec(memory_space=pltpu.VMEM)
-    hbm = pl.BlockSpec(memory_space=pl.ANY)
-    return pl.pallas_call(
+    hbm = pl.BlockSpec(memory_space=pltpu.HBM)
+    call = pl.pallas_call(
         functools.partial(exchange, n),
         out_shape=(
-            jax.ShapeDtypeStruct((count, width), jnp.bfloat16),
-            jax.ShapeDtypeStruct(quarter, jnp.bfloat16),
+            pltpu.VMEM((count, width), jnp.bfloat16),
+            pltpu.VMEM(quarter, jnp.bfloat16),
         ),
-        in_specs=[vmem] * 7 + [pl.BlockSpec(memory_space=pltpu.SMEM)] + [hbm] * 7,
+        in_specs=[hbm] * 15,
         out_specs=(vmem, vmem),
         scratch_shapes=[
+            pltpu.VMEM(tokens_in.shape, jnp.bfloat16),
+            pltpu.VMEM((1, width), jnp.float32),
+            pltpu.VMEM((TOP, count), jnp.int32),
+            pltpu.VMEM((TOP, count), jnp.float32),
+            pltpu.VMEM(queries_a.shape, jnp.bfloat16),
+            pltpu.VMEM(queries_b.shape, jnp.bfloat16),
+            pltpu.VMEM((1, VDIM), jnp.float32),
+            pltpu.SMEM(lambdas.shape, jnp.float32),
             pltpu.VMEM(block, jnp.bfloat16),
             pltpu.VMEM(block, jnp.bfloat16),
-            pltpu.VMEM((2, n, cap, count), jnp.bfloat16),
+            pltpu.VMEM((2, count, n * cap), jnp.bfloat16),
             pltpu.VMEM((n, 4, cap, width), jnp.bfloat16),
             pltpu.VMEM((n, 4, cap, width), jnp.bfloat16),
             pltpu.VMEM(block, jnp.bfloat16),
@@ -572,17 +600,19 @@
             pltpu.VMEM(quarter, jnp.bfloat16),
             pltpu.SemaphoreType.DMA((11, n)),
             pltpu.SemaphoreType.DMA((11, n)),
-            pltpu.SemaphoreType.DMA((7,)),
+            pltpu.SemaphoreType.DMA((15,)),
         ],
         compiler_params=pltpu.CompilerParams(
-            collective_id=0, has_side_effects=True, vmem_limit_bytes=60 * 2**20
+            collective_id=0, has_side_effects=True, vmem_limit_bytes=48 * 2**20
         ),
         name="exchange",
-    )(
+    )
+    operands = (
         tokens_in, moe_gain.reshape(1, -1), routes.T, route_weights.T,
         queries_a, queries_b, head_gain.reshape(1, -1), lambdas,
         keys_a, keys_b, values, w_gate, w_up, w_down, w_out,
     )
+    return call(*[pltpu.with_memory_space_constraint(x, pltpu.HBM) for x in operands])
 
 
 def fast_body(
@@ -602,7 +632,7 @@
     n, n_tp = lax.axis_size("ep"), lax.axis_size("tp")
     tok_rows, w_gate = args[8].shape[0], args[12]
     cap = 3 * tok_rows * TOP // (2 * n)
-    if w_gate.shape[0] == 1 and n_tp == 4 and n & (n - 1) == 0 and n >= 8 and cap % 16 == 0:
+    if w_gate.shape[0] == 1 and n_tp == 4 and n == 8 and cap % 16 == 0:
         return fast_body(*args)
     return body(*args)
 

time: 105 us -> 93.9 us (0.89)
  the two profiles are of different devices: /device:TPU:16 before, /device:TPU:0 now
where the time goes in v2:
time: 93.9 us; the launch traced here: 93.8 us
  Pallas kernels  91.7 us (98%)
  local copies, waits for them, and re-layouts  1.45 us (2%)
    pallas_call x1, Pallas kernels, run_exchange(): call(*[pltpu.with_memory_space_constraint(x, pltpu.HBM) for x in operands])  91.7 us

profile of v2, /device:TPU:0, one launch (start us, length us, event | category | flops | bytes accessed | tf_op | source)
XLA Modules:
  0.0 93.8 jit_solution(14723954519404576273)
XLA Ops:
  0.6 91.7 %exchange.1 = (bf16[128,2048]{1,0:T(8,128)(2,1)S(1)}, bf16[32,2048]{1,0:T(8,128)(2,1)S(1)}) custom-call(bf16[128,2048]{1,0:T(8,128)(2,1)} %moe_tokens.1, f32[1,2048]{1,0:T(1,128)} %bitcast.10, s32[2,128]{1,0:T(2,128)} %bitcast.11, f32[2,128]{1,0:T(2,128)} %bitcast.12, bf16[128,256]{1,0:T(8,128)(2,1)} %queries_a_in.1, bf16[128,256]{1,0:T(8,128)(2,1)} %queries_b_in.1, ...), custom_call_target="tpu_custom_call" | custom-call | tf_op jit(solution)/shard_map/exchange/pallas_call | solution.py:615
  92.3 0.7 copy.19
  93.0 0.8 copy.20

commit v3 on v2

--- a/solution.py
+++ b/solution.py
@@ -162,7 +162,7 @@
 
 
 MESH = pl.DeviceIdType.MESH
-OUT, CORE, ACROSS, CORE_ACROSS, PART, PAIR, SUMS, BACK, KV_Z, KV_Y, MIX = range(11)
+OUT, ACROSS, CORE, PAIR, PART, KV_Z, KV_Y, MIX, BACK, RELAYS, HALVES, TRIPS = range(12)
 
 
 def xor(first, second, limit):
@@ -178,7 +178,7 @@
     keys_a, keys_b, values, w_gate, w_up, w_down, w_out,
     moe_out, mixer_out,
     tokens_in, moe_gain, routes, route_weights, queries_a, queries_b, head_gain, lambdas,
-    ret, outgoing, weigh, rows, parts, part_in, pair_in, sums_in, sums, final, hidden, gate_v, up_v, down_v, out_v,
+    ret, outgoing, weigh, rows, parts, part_in, pair_in, sums, final, hidden, gate_v, up_v, down_v, out_v,
     kv_all, heads, shares, mix_part, mix_pair, mix_in, mix_sum, send, recv, local,
 ):
     me = lax.axis_index("ep")
@@ -193,58 +193,82 @@
     flat = 4 * cap
     tokens = kv_all.shape[1]
 
-    def mask_of(k):
-        far = k // 2
-        return 2 * ((far + 1) % 3 + 1) * ((far + 3) // 4) + k % 2
+    inner = (floor + 1) // 2 % 2
+
+    def order(step):
+        turn = step // 2
+        return step + inner * (2 * (turn // 2 + 2 * (turn % 2)) + step % 2 - step)
 
     def partner(k):
-        return xor(me, mask_of(k), n)
-
-    def copy(kind, k, source, target, device):
+        return xor(me, k, n)
+
+    def place_of(kind, k):
+        return n * kind + k if kind < KV_Z else 5 * n + 4 * (kind - KV_Z) + k
+
+    def sent_by(kind, k):
+        return kind - BACK if kind > BACK else 3 + 4 * (kind - KV_Z) + k
+
+    def copy(kind, k, group, source, target, device):
         return pltpu.make_async_remote_copy(
             src_ref=source,
             dst_ref=target,
-            send_sem=send.at[kind, k],
-            recv_sem=recv.at[kind, k],
+            send_sem=send.at[sent_by(group, k)],
+            recv_sem=recv.at[place_of(kind, k)],
             device_id=device,
             device_id_type=MESH,
         )
 
     def out_copy(k):
-        return copy(OUT, k, outgoing.at[partner(k)], rows.at[k, 0], {"ep": partner(k)})
+        return copy(OUT, k, TRIPS, outgoing.at[partner(k)], rows.at[k, 0], {"ep": partner(k)})
 
     def core_copy(k):
-        return copy(CORE, k, rows.at[k, 0], rows.at[k, 1], {"tp": core})
+        return copy(CORE, k, RELAYS, rows.at[k, 0], rows.at[k, 1], {"tp": core})
 
     def across_copy(k):
-        return copy(ACROSS, k, rows.at[k, 0], rows.at[k, 2], {"tp": across})
+        return copy(ACROSS, k, RELAYS, rows.at[k, 0], rows.at[k, 2], {"tp": across})
 
     def core_across_copy(k):
-        return copy(CORE_ACROSS, k, rows.at[k, 2], rows.at[k, 3], {"tp": core})
+        return copy(CORE, k, RELAYS, rows.at[k, 2], rows.at[k, 3], {"tp": core})
+
+    def both_core_copies(k):
+        return copy(CORE, k, RELAYS, rows.at[k, 0:2], rows.at[k, 2:4], {"tp": core})
 
     def part_copy(k):
-        return copy(PART, k, parts.at[k, 1], part_in.at[k], {"tp": core})
+        return copy(PART, k, HALVES, parts.at[k, 1], part_in.at[0, k], {"tp": core})
 
     def pair_copy(k):
-        return copy(PAIR, k, parts.at[k, 3], pair_in.at[k], {"tp": core})
+        return copy(PAIR, k, HALVES, parts.at[k, 3], pair_in.at[k], {"tp": core})
 
     def sums_copy(k):
-        return copy(SUMS, k, sums.at[k], sums_in.at[k], {"tp": across})
+        return copy(PART, k, RELAYS, sums.at[k], part_in.at[1, k], {"tp": across})
+
+    def part_and_sums(k):
+        return copy(PART, k, RELAYS, rows.at[k, 0:2], part_in.at[:, k], {"tp": across})
 
     def back_copy(k):
-        return copy(BACK, k, final.at[k], ret.at[me], {"ep": partner(k)})
+        return copy(BACK, 0, TRIPS, final.at[k], ret.at[me], {"ep": partner(k)})
+
+    def all_back():
+        return copy(BACK, 0, TRIPS, final.at[0 : n - 1], ret.at[0 : n - 1], {"tp": core})
+
+    def all_sent():
+        return [
+            copy(OUT, 0, RELAYS, rows, rows, {"tp": core}),
+            copy(OUT, 0, HALVES, rows.at[:, 0:2], rows.at[:, 0:2], {"tp": core}),
+            copy(OUT, 0, TRIPS, rows.at[0 : n - 1, 0:2], rows.at[0 : n - 1, 0:2], {"tp": core}),
+        ]
 
     def kv_z_copy(stage):
         block = kv_all.at[2 * (floor - stage + 1) + lane]
-        return copy(KV_Z, stage, block, block, {"ep": me + 2})
+        return copy(KV_Z, stage, KV_Z, block, block, {"ep": me + 2})
 
     def kv_y_copy(stage):
         block = kv_all.at[2 * (floor - stage) + lane]
-        return copy(KV_Y, stage, block, block, {"ep": me + 1 - 2 * lane})
-
-    mix_part_copy = copy(MIX, 0, shares.at[core], mix_part, {"tp": core})
-    mix_pair_copy = copy(MIX, 1, shares.at[diagonal], mix_pair, {"tp": core})
-    mix_sum_copy = copy(MIX, 2, mix_sum, mix_in, {"tp": across})
+        return copy(KV_Y, stage, KV_Y, block, block, {"ep": me + 1 - 2 * lane})
+
+    mix_part_copy = copy(MIX, 0, MIX, shares.at[core], mix_part, {"tp": core})
+    mix_pair_copy = copy(MIX, 1, MIX, shares.at[diagonal], mix_pair, {"tp": core})
+    mix_sum_copy = copy(MIX, 2, MIX, mix_sum, mix_in, {"tp": across})
 
     local_heads = heads.shape[1] // VDIM
     kv_local = kv_all.shape[2] // (2 * HEAD + VDIM)
@@ -296,12 +320,11 @@
         sums_copy(k).start()
 
     def finish(k):
-        part_copy(k).wait_recv()
-        sums_copy(k).wait_recv()
+        part_and_sums(k).wait_recv()
         return (
             parts[k, 0].astype(jnp.float32)
-            + part_in[k].astype(jnp.float32)
-            + sums_in[k].astype(jnp.float32)
+            + part_in[0, k].astype(jnp.float32)
+            + part_in[1, k].astype(jnp.float32)
         ).astype(jnp.bfloat16)
 
     def send_back(k):
@@ -309,8 +332,7 @@
         back_copy(k).start()
 
     def feed(k):
-        core_copy(k).wait_recv()
-        core_across_copy(k).wait_recv()
+        both_core_copies(k).wait_recv()
         inputs = rows[k].reshape(flat, width)
         step = min(256, units)
         for first in range(0, units, step):
@@ -389,26 +411,18 @@
     pl.semaphore_wait(barrier, n + 2)
 
     forward(0)
-    for k in range(1, n // 2):
+    for k in (1, 4, 2):
         out_copy(k).start()
+
+    for other in range(1, floors):
+
+        @pl.when(floor < other)
+        def _():
+            for side in range(2):
+                kv_all[2 * other + side] = jnp.zeros(kv_all.shape[1:], jnp.bfloat16)
+
     for load in loads[3:7]:
         load.wait()
-
-    @pl.when(floor < floors - 1)
-    def _():
-        kv_z_copy(1).start()
-
-    for k in range(n // 2, n):
-        out_copy(k).start()
-    kv_y_copy(0).start()
-
-    for other in range(1, floors):
-
-        @pl.when(floor < other)
-        def _():
-            for side in range(2):
-                kv_all[2 * other + side] = jnp.zeros(kv_all.shape[1:], jnp.bfloat16)
-
     share = route_weights[...]
     scale = jnp.where(named[0], share[0:1, :], 0.0)
     for k in range(1, TOP):
@@ -423,6 +437,7 @@
     high = table.astype(jnp.bfloat16)
     weigh[0] = high
     weigh[1] = (table - high.astype(jnp.float32)).astype(jnp.bfloat16)
+    out_copy(5).start()
     for load in loads[7:]:
         load.wait()
 
@@ -437,44 +452,83 @@
                 def _():
                     kv_z_copy(stage + 1).start()
 
+    def pass_on(k):
+        out_copy(k).wait_recv()
+        forward(k)
+
     @pl.loop(0, n)
-    def _(k):
-        @pl.when((k >= 2) & (k < 4))
-        def _():
-            send_sums(k - 1)
-
-        @pl.when(k + 1 < n)
-        def _():
-            out_copy(k + 1).wait_recv()
-            forward(k + 1)
-
-        @pl.when(k == 4)
-        def _():
-            send_sums(3)
+    def _(step):
+        @pl.when(step == 3)
+        def _():
+            send_sums(1)
+
+        @pl.when(step < 5)
+        def _():
+            pass_on(order(step + 1))
+
+        for k in (6, 7):
+
+            @pl.when(step == k - 2 + inner)
+            def _():
+                pass_on(k)
+
+        for k in (4, 5):
+
+            @pl.when(step == k + 2 - inner)
+            def _():
+                send_sums(k)
+
+        @pl.when(step == 0)
+        def _():
+            out_copy(3).start()
+            out_copy(6).start()
+
+        @pl.when(step == 1)
+        def _():
+            out_copy(7).start()
+
+        @pl.when(step == 2)
+        def _():
+            @pl.when(floor < floors - 1)
+            def _():
+                kv_z_copy(1).start()
+
+            kv_y_copy(0).start()
+
+        @pl.when(step == 5)
+        def _():
             send_back(1)
+
+        @pl.when(step == 6)
+        def _():
             kv_next(1)
 
-        @pl.when(k == 5)
-        def _():
-            send_back(2)
-
-        @pl.when(k == 6)
-        def _():
-            send_sums(4)
-            send_back(3)
+        @pl.when((step == 7) & (inner == 1))
+        def _():
+            send_sums(6)
+            send_back(4)
+
+        @pl.when(step == 7)
+        def _():
             kv_next(2)
 
-        @pl.when(k == 7)
-        def _():
-            send_sums(6)
-            kv_next(3)
-
-        relay(k)
-        feed(k)
+        relay(order(step))
+        feed(order(step))
+
+    @pl.when(inner == 0)
+    def _():
+        send_sums(6)
 
     send_sums(7)
-    send_back(4)
-    send_sums(5)
+
+    @pl.when(inner == 0)
+    def _():
+        send_back(4)
+
+    send_back(5)
+    send_sums(2)
+    send_sums(3)
+    kv_next(3)
     for stage in range(floors):
 
         @pl.when(floor >= stage)
@@ -493,20 +547,18 @@
         )
     mix_pair_copy.start()
     mix_part_copy.start()
+    send_back(7)
     mix_pair_copy.wait_recv()
     mix_sum[...] = (
         shares[across].astype(jnp.float32) + mix_pair[...].astype(jnp.float32)
     ).astype(jnp.bfloat16)
     mix_sum_copy.start()
     send_sums(0)
-    send_back(7)
-    send_back(5)
+    send_back(2)
+    send_back(3)
     ret[me] = finish(0)
 
-    @pl.loop(1, n)
-    def _(k):
-        back_copy(k).wait_recv()
-
+    all_back().wait_recv()
     for first in range(0, width, 256):
         table = ret[:, :, first : first + 256].reshape(n * cap, 256)
         total = jnp.dot(weigh[0], table, preferred_element_type=jnp.float32) + jnp.dot(
@@ -536,15 +588,8 @@
         def _():
             kv_y_copy(stage).wait_send()
 
-    @pl.loop(0, n)
-    def _(k):
-        for made in (core_copy, across_copy, core_across_copy, part_copy, pair_copy, sums_copy):
-            made(k).wait_send()
-
-        @pl.when(k >= 1)
-        def _():
-            out_copy(k).wait_send()
-            back_copy(k).wait_send()
+    for made in all_sent():
+        made.wait_send()
 
 
 def run_exchange(
@@ -581,8 +626,7 @@
             pltpu.VMEM((2, count, n * cap), jnp.bfloat16),
             pltpu.VMEM((n, 4, cap, width), jnp.bfloat16),
             pltpu.VMEM((n, 4, cap, width), jnp.bfloat16),
-            pltpu.VMEM(block, jnp.bfloat16),
-            pltpu.VMEM(block, jnp.bfloat16),
+            pltpu.VMEM((2,) + block, jnp.bfloat16),
             pltpu.VMEM(block, jnp.bfloat16),
             pltpu.VMEM(block, jnp.bfloat16),
             pltpu.VMEM(block, jnp.bfloat16),
@@ -598,8 +642,8 @@
             pltpu.VMEM(quarter, jnp.bfloat16),
             pltpu.VMEM(quarter, jnp.bfloat16),
             pltpu.VMEM(quarter, jnp.bfloat16),
-            pltpu.SemaphoreType.DMA((11, n)),
-            pltpu.SemaphoreType.DMA((11, n)),
+            pltpu.SemaphoreType.DMA((15,)),
+            pltpu.SemaphoreType.DMA((5 * n + 13,)),
             pltpu.SemaphoreType.DMA((15,)),
         ],
         compiler_params=pltpu.CompilerParams(

time: 93.9 us -> 89.3 us (0.951)
  Pallas kernels: 91.7 us -> 87 us
    pallas_call x1, Pallas kernels: 91.7 us -> 87 us  [run_exchange(): call(*[pltpu.with_memory_space_constraint(x, pltpu.HBM) for x in operands])]
where the time goes in v3:
time: 89.3 us; the launch traced here: 89.1 us
  Pallas kernels  87 us (97%)
  local copies, waits for them, and re-layouts  1.45 us (2%)
    pallas_call x1, Pallas kernels, run_exchange(): call(*[pltpu.with_memory_space_constraint(x, pltpu.HBM) for x in operands])  87 us

profile of v3, /device:TPU:0, one launch (start us, length us, event | category | flops | bytes accessed | tf_op | source)
XLA Modules:
  0.0 89.1 jit_solution(256632621762182937)
XLA Ops:
  0.6 87.0 %exchange.1 = (bf16[128,2048]{1,0:T(8,128)(2,1)S(1)}, bf16[32,2048]{1,0:T(8,128)(2,1)S(1)}) custom-call(bf16[128,2048]{1,0:T(8,128)(2,1)} %moe_tokens.1, f32[1,2048]{1,0:T(1,128)} %bitcast.10, s32[2,128]{1,0:T(2,128)} %bitcast.11, f32[2,128]{1,0:T(2,128)} %bitcast.12, bf16[128,256]{1,0:T(8,128)(2,1)} %queries_a_in.1, bf16[128,256]{1,0:T(8,128)(2,1)} %queries_b_in.1, ...), custom_call_target="tpu_custom_call" | custom-call | tf_op jit(solution)/shard_map/exchange/pallas_call | solution.py:659
  87.7 0.7 copy.19
  88.3 0.8 copy.20

commit v4 on v3

--- a/solution.py
+++ b/solution.py
@@ -411,8 +411,9 @@
     pl.semaphore_wait(barrier, n + 2)
 
     forward(0)
-    for k in (1, 4, 2):
+    for k in (1, 4):
         out_copy(k).start()
+    out_copy(5 - 3 * inner).start()
 
     for other in range(1, floors):
 
@@ -435,9 +436,9 @@
         axis=0,
     ).T
     high = table.astype(jnp.bfloat16)
-    weigh[0] = high
-    weigh[1] = (table - high.astype(jnp.float32)).astype(jnp.bfloat16)
-    out_copy(5).start()
+    weigh[0:count] = high
+    weigh[count:] = (table - high.astype(jnp.float32)).astype(jnp.bfloat16)
+    out_copy(2 + 3 * inner).start()
     for load in loads[7:]:
         load.wait()
 
@@ -526,8 +527,8 @@
         send_back(4)
 
     send_back(5)
+    send_sums(3)
     send_sums(2)
-    send_sums(3)
     kv_next(3)
     for stage in range(floors):
 
@@ -554,17 +555,15 @@
     ).astype(jnp.bfloat16)
     mix_sum_copy.start()
     send_sums(0)
+    send_back(3)
     send_back(2)
-    send_back(3)
     ret[me] = finish(0)
 
     all_back().wait_recv()
     for first in range(0, width, 256):
         table = ret[:, :, first : first + 256].reshape(n * cap, 256)
-        total = jnp.dot(weigh[0], table, preferred_element_type=jnp.float32) + jnp.dot(
-            weigh[1], table, preferred_element_type=jnp.float32
-        )
-        moe_out[:, first : first + 256] = total.astype(jnp.bfloat16)
+        total = jnp.dot(weigh[...], table, preferred_element_type=jnp.float32)
+        moe_out[:, first : first + 256] = (total[:count] + total[count:]).astype(jnp.bfloat16)
 
     mix_part_copy.wait_recv()
     mix_sum_copy.wait_recv()
@@ -590,6 +589,17 @@
 
     for made in all_sent():
         made.wait_send()
+
+
+def settle(first, second, first_out, second_out, sems):
+    copies = [
+        pltpu.make_async_copy(first, first_out, sems.at[0]),
+        pltpu.make_async_copy(second, second_out, sems.at[1]),
+    ]
+    for made in copies:
+        made.start()
+    for made in copies:
+        made.wait()
 
 
 def run_exchange(
@@ -623,7 +633,7 @@
             pltpu.SMEM(lambdas.shape, jnp.float32),
             pltpu.VMEM(block, jnp.bfloat16),
             pltpu.VMEM(block, jnp.bfloat16),
-            pltpu.VMEM((2, count, n * cap), jnp.bfloat16),
+            pltpu.VMEM((2 * count, n * cap), jnp.bfloat16),
             pltpu.VMEM((n, 4, cap, width), jnp.bfloat16),
             pltpu.VMEM((n, 4, cap, width), jnp.bfloat16),
             pltpu.VMEM((2,) + block, jnp.bfloat16),
@@ -656,7 +666,16 @@
         queries_a, queries_b, head_gain.reshape(1, -1), lambdas,
         keys_a, keys_b, values, w_gate, w_up, w_down, w_out,
     )
-    return call(*[pltpu.with_memory_space_constraint(x, pltpu.HBM) for x in operands])
+    made = call(*[pltpu.with_memory_space_constraint(x, pltpu.HBM) for x in operands])
+    return pl.pallas_call(
+        settle,
+        out_shape=tuple(jax.ShapeDtypeStruct(x.shape, x.dtype) for x in made),
+        in_specs=[vmem] * 2,
+        out_specs=(hbm, hbm),
+        scratch_shapes=[pltpu.SemaphoreType.DMA((2,))],
+        compiler_params=pltpu.CompilerParams(vmem_limit_bytes=2**20),
+        name="settle",
+    )(*[pltpu.with_memory_space_constraint(x, pltpu.VMEM) for x in made])
 
 
 def fast_body(

time: 89.3 us -> 87.2 us (0.976)
  local copies, waits for them, and re-layouts: 1.45 us -> 0 us
    pallas_call x1, Pallas kernels: 87 us -> 85.5 us  [run_exchange(): call(*[pltpu.with_memory_space_constraint(x, pltpu.HBM) for x in operands])]
    unnamed x2 -> x0, local copies, waits for them, and re-layouts: 1.45 us -> none
where the time goes in v4:
time: 87.2 us; the launch traced here: 87 us
  Pallas kernels  86.4 us (99%)
    pallas_call x1, Pallas kernels, run_exchange(): call(*[pltpu.with_memory_space_constraint(x, pltpu.HBM) for x in operands])  85.5 us

profile of v4, /device:TPU:0, one launch (start us, length us, event | category | flops | bytes accessed | tf_op | source)
XLA Modules:
  0.0 87.0 jit_solution(9517915084866466799)
XLA Ops:
  0.6 85.5 %exchange.1 = (bf16[128,2048]{1,0:T(8,128)(2,1)S(1)}, bf16[32,2048]{1,0:T(8,128)(2,1)S(1)}) custom-call(bf16[128,2048]{1,0:T(8,128)(2,1)} %moe_tokens.1, f32[1,2048]{1,0:T(1,128)} %bitcast.10, s32[2,128]{1,0:T(2,128)} %bitcast.11, f32[2,128]{1,0:T(2,128)} %bitcast.12, bf16[128,256]{1,0:T(8,128)(2,1)} %queries_a_in.1, bf16[128,256]{1,0:T(8,128)(2,1)} %queries_b_in.1, ...), custom_call_target="tpu_custom_call" | custom-call | tf_op jit(solution)/shard_map/exchange/pallas_call | solution.py:669
  86.2 0.8 settle.1

commit v5 on v4

--- a/solution.py
+++ b/solution.py
@@ -475,7 +475,7 @@
 
         for k in (4, 5):
 
-            @pl.when(step == k + 2 - inner)
+            @pl.when(step == k + 1)
             def _():
                 send_sums(k)
 
@@ -488,7 +488,7 @@
         def _():
             out_copy(7).start()
 
-        @pl.when(step == 2)
+        @pl.when(step == 3)
         def _():
             @pl.when(floor < floors - 1)
             def _():
@@ -536,9 +536,9 @@
         def _():
             kv_y_copy(stage).wait_recv()
 
+    send_back(6)
     for head in range(local_heads):
         attend(head)
-    send_back(6)
     for first in range(0, width, 256):
         piece = jnp.dot(
             heads[...], out_v[:, first : first + 256], preferred_element_type=jnp.float32

time: 87.2 us -> 87.1 us (level)
  no operation moved by 1% of the time
where the time goes in v5:
time: 87.1 us; the launch traced here: 86.9 us
  Pallas kernels  86.3 us (99%)
    pallas_call x1, Pallas kernels, run_exchange(): call(*[pltpu.with_memory_space_constraint(x, pltpu.HBM) for x in operands])  85.4 us

profile of v5, /device:TPU:0, one launch (start us, length us, event | category | flops | bytes accessed | tf_op | source)
XLA Modules:
  0.0 86.9 jit_solution(12084659274223993531)
XLA Ops:
  0.6 85.4 %exchange.1 = (bf16[128,2048]{1,0:T(8,128)(2,1)S(1)}, bf16[32,2048]{1,0:T(8,128)(2,1)S(1)}) custom-call(bf16[128,2048]{1,0:T(8,128)(2,1)} %moe_tokens.1, f32[1,2048]{1,0:T(1,128)} %bitcast.10, s32[2,128]{1,0:T(2,128)} %bitcast.11, f32[2,128]{1,0:T(2,128)} %bitcast.12, bf16[128,256]{1,0:T(8,128)(2,1)} %queries_a_in.1, bf16[128,256]{1,0:T(8,128)(2,1)} %queries_b_in.1, ...), custom_call_target="tpu_custom_call" | custom-call | tf_op jit(solution)/shard_map/exchange/pallas_call | solution.py:669
  86.1 0.8 settle.1
